TPU v7x, 32 devices: a whole 2x2x4 slice. The times are simulated.
32 devices in a mesh: sp: 8 (over z, y), tp: 4 (over x, core).
Axes of the slice: x: 2, y: 2, z: 4, core: 2. Of those that a mesh axis runs over, the one named last changes fastest.
Arguments:
- resid: bfloat16 [2048, 2048], P(('sp', 'tp')), may hold values from -6 to 6
- query_a: bfloat16 [2048, 4, 128], P('sp', 'tp')
- key_a: bfloat16 [2048, 4, 128], P('sp', 'tp')
- value_a: bfloat16 [2048, 4, 128], P('sp', 'tp'), may hold values from -6 to 6
- query_b: bfloat16 [2048, 4, 256], P('sp', 'tp')
- key_b: bfloat16 [2048, 4, 256], P('sp', 'tp')
- value_b: bfloat16 [2048, 4, 128], P('sp', 'tp'), may hold values from -6 to 6
- lambda_a: float32 [4], P('tp'), may hold values from 0.3 to 0.8
- lambda_b: float32 [4], P('tp'), may hold values from 0.3 to 0.8
- head_gain: float32 [128], replicated, may hold values from 0.1 to 1.9
- out_weight: bfloat16 [1024, 2048], replicated, may hold values from -0.1875 to 0.1875
- norm_gain: float32 [2048], replicated, may hold values from 0.1 to 1.9
- expert_ids: int32 [2048, 4], P(('sp', 'tp')), may hold values from 0 to 31, all different within a row; in each aligned block of 64 rows (0 to 63, 64 to 127, ...) at most 16 rows name the same one
- expert_mix: float32 [2048, 4], P(('sp', 'tp')), may hold values from 0.2 to 1
- gate_experts: bfloat16 [32, 2048, 1024], P(('sp', 'tp')), may hold values from -0.125 to 0.125
- up_experts: bfloat16 [32, 2048, 1024], P(('sp', 'tp')), may hold values from -0.125 to 0.125
- down_experts: bfloat16 [32, 1024, 2048], P(('sp', 'tp')), may hold values from -0.1875 to 0.1875
- shared_gate: bfloat16 [2048, 512], replicated, may hold values from -0.125 to 0.125
- shared_up: bfloat16 [2048, 512], replicated, may hold values from -0.125 to 0.125
- shared_down: bfloat16 [512, 2048], replicated, may hold values from -0.25 to 0.25
Outputs:
- layer_out: bfloat16 [2048, 2048], P(('sp', 'tp'))
Inputs may be any that keep to these rules, and one draw needn't show every extreme that they name: `expert_ids`: in each aligned block of 64 rows (the rows of one device) no expert is named more than 16 times, a bound that some block reaches.
All inputs are finite; a program needn't handle non-finite values.
Results may differ from a plain program's by a relative error of at most 0.017.
Values may be sent and summed in bfloat16 or wider, within the bound.
No kernel may reach another device: no remote copies, remote signals or barrier semaphores. Data moves between devices by JAX's collectives and lax.ppermute only.
A program may use at most 128 MiB of HBM per device.

v0:
```python
import math
import jax
import jax.numpy as jnp
from jax import lax
from jax.sharding import PartitionSpec as P

NEG_FILL = -1e30
EPSILON = 1e-05
HEAD_SCALE = 0.8
KEY_SPAN = 2048


def swiglu_rows(row_set, w_gate, w_up, w_down):
    gate_val = jnp.dot(row_set, w_gate, preferred_element_type=jnp.float32)
    up_val = jnp.dot(row_set, w_up, preferred_element_type=jnp.float32)
    hidden = (jax.nn.silu(gate_val) * up_val).astype(jnp.bfloat16)
    return jnp.dot(hidden, w_down, preferred_element_type=jnp.float32)


def online_update(state, query_map, key_map, value_block, causal, scaling):
    row_top, denoms, numerator = state
    scores = (
        jnp.einsum("qhd,khd->hqk", query_map, key_map, preferred_element_type=jnp.float32) * scaling
    )
    scores = jnp.where(causal, scores, NEG_FILL)
    new_top = jnp.maximum(row_top, jnp.max(scores, axis=2))
    exponent = jnp.where(causal, jnp.exp(scores - new_top[:, :, None]), 0.0)
    shrink = jnp.exp(row_top - new_top)
    denoms = denoms * shrink + jnp.sum(exponent, axis=2)
    numerator = numerator * jnp.transpose(shrink)[:, :, None] + jnp.einsum(
        "hqk,khe->qhe",
        exponent.astype(jnp.bfloat16),
        value_block,
        preferred_element_type=jnp.float32,
    )
    return (new_top, denoms, numerator)


def group_update(states, queries, key_block, value_block, causal):
    map_width = queries.shape[2] // 2
    scaling = map_width ** (-0.5)
    first_state = online_update(
        states[0],
        queries[:, :, :map_width],
        key_block[:, :, :map_width],
        value_block,
        causal,
        scaling,
    )
    second_state = online_update(
        states[1],
        queries[:, :, map_width:],
        key_block[:, :, map_width:],
        value_block,
        causal,
        scaling,
    )
    return (first_state, second_state)


def empty_state(query_rows, head_count, value_width):
    single = (
        jnp.full((head_count, query_rows), NEG_FILL, jnp.float32),
        jnp.zeros((head_count, query_rows), jnp.float32),
        jnp.zeros((query_rows, head_count, value_width), jnp.float32),
    )
    return (single, single)


def finish_group(states, lambdas, head_gain):
    first_out = states[0][2] / jnp.transpose(states[0][1])[:, :, None]
    second_out = states[1][2] / jnp.transpose(states[1][1])[:, :, None]
    differ = first_out - lambdas[None, :, None] * second_out
    scale_rms = lax.rsqrt(jnp.mean(differ * differ, axis=2, keepdims=True) + EPSILON)
    return (differ * scale_rms * head_gain[None, None, :] * HEAD_SCALE).astype(jnp.bfloat16)


def per_device(
    resid,
    query_a,
    key_a,
    value_a,
    query_b,
    key_b,
    value_b,
    lambda_a,
    lambda_b,
    head_gain,
    out_weight,
    norm_gain,
    expert_ids,
    expert_mix,
    gate_experts,
    up_experts,
    down_experts,
    shared_gate,
    shared_up,
    shared_down,
):
    query_rows = query_a.shape[0]
    value_width = value_a.shape[2]
    query_pos = lax.axis_index("sp") * query_rows + jnp.arange(query_rows, dtype=jnp.int32)
    start_state = (
        empty_state(query_rows, query_a.shape[1], value_width),
        empty_state(query_rows, query_b.shape[1], value_width),
    )
    key_piece_a = lax.all_gather(key_a, "sp", axis=0, tiled=True)
    value_piece_a = lax.all_gather(value_a, "sp", axis=0, tiled=True)
    key_piece_b = lax.all_gather(key_b, "sp", axis=0, tiled=True)
    value_piece_b = lax.all_gather(value_b, "sp", axis=0, tiled=True)
    piece_rows = key_piece_a.shape[0]
    step_rows = math.gcd(piece_rows, KEY_SPAN)

    def one_step(step_index, inner_state):
        begin_row = step_index * step_rows
        key_pos = begin_row + jnp.arange(step_rows, dtype=jnp.int32)
        causal = (key_pos[None, :] <= query_pos[:, None])[None]
        part_a = group_update(
            inner_state[0],
            query_a,
            lax.dynamic_slice_in_dim(key_piece_a, begin_row, step_rows, 0),
            lax.dynamic_slice_in_dim(value_piece_a, begin_row, step_rows, 0),
            causal,
        )
        part_b = group_update(
            inner_state[1],
            query_b,
            lax.dynamic_slice_in_dim(key_piece_b, begin_row, step_rows, 0),
            lax.dynamic_slice_in_dim(value_piece_b, begin_row, step_rows, 0),
            causal,
        )
        return (part_a, part_b)

    state_a, state_b = lax.fori_loop(0, piece_rows // step_rows, one_step, start_state)
    heads_a = finish_group(state_a, lambda_a, head_gain)
    heads_b = finish_group(state_b, lambda_b, head_gain)
    tok_dev = resid.shape[0]
    back_a, back_b = (
        lax.all_to_all(heads_a, "tp", split_axis=0, concat_axis=1, tiled=True),
        lax.all_to_all(heads_b, "tp", split_axis=0, concat_axis=1, tiled=True),
    )
    joined = jnp.concatenate([back_a.reshape(tok_dev, -1), back_b.reshape(tok_dev, -1)], axis=1)
    project = jnp.dot(joined, out_weight, preferred_element_type=jnp.float32)
    middle = (resid.astype(jnp.float32) + project).astype(jnp.bfloat16)
    middle_f = middle.astype(jnp.float32)
    normed = (
        middle_f
        * lax.rsqrt(jnp.mean(middle_f * middle_f, axis=1, keepdims=True) + EPSILON)
        * norm_gain[None, :]
    ).astype(jnp.bfloat16)
    shared = swiglu_rows(normed, shared_gate, shared_up, shared_down)
    top_count = expert_ids.shape[1]
    model_width = normed.shape[1]
    sp_count = lax.axis_size("sp")
    tp_count = lax.axis_size("tp")
    expert_total = sp_count * tp_count
    pair_count = tok_dev * top_count
    capacity = max(2, 2 * pair_count // expert_total)
    flat_ids = expert_ids.reshape(-1)
    one_hot = (flat_ids[:, None] == jnp.arange(expert_total, dtype=jnp.int32)[None, :]).astype(
        jnp.int32
    )
    pair_rank = jnp.sum((jnp.cumsum(one_hot, axis=0) - one_hot) * one_hot, axis=1)
    pair_token = jnp.arange(pair_count, dtype=jnp.int32) // top_count
    send_rows = (
        jnp.zeros((expert_total, capacity, model_width), jnp.bfloat16)
        .at[flat_ids, pair_rank]
        .set(normed[pair_token])
    )
    arrived = lax.all_to_all(send_rows, ("sp", "tp"), split_axis=0, concat_axis=0, tiled=True)
    arrived_shape = arrived.shape
    flat_rows = arrived.reshape(-1, arrived_shape[-1])
    result = swiglu_rows(flat_rows, gate_experts[0], up_experts[0], down_experts[0]).astype(
        jnp.bfloat16
    )
    finished = result.reshape(arrived_shape)
    returned = lax.all_to_all(finished, ("sp", "tp"), split_axis=0, concat_axis=0, tiled=True)
    chosen = returned[flat_ids, pair_rank].reshape(tok_dev, top_count, model_width)
    routed = jnp.sum(chosen.astype(jnp.float32) * expert_mix[:, :, None], axis=1)
    return (middle_f + shared + routed).astype(jnp.bfloat16)


def solution(mesh):
    in_specs = (
        P(("sp", "tp"), None),
        P("sp", "tp", None),
        P("sp", "tp", None),
        P("sp", "tp", None),
        P("sp", "tp", None),
        P("sp", "tp", None),
        P("sp", "tp", None),
        P("tp"),
        P("tp"),
        P(),
        P(),
        P(),
        P(("sp", "tp"), None),
        P(("sp", "tp"), None),
        P(("sp", "tp"), None, None),
        P(("sp", "tp"), None, None),
        P(("sp", "tp"), None, None),
        P(),
        P(),
        P(),
    )
    out_specs = P(("sp", "tp"), None)
    return jax.shard_map(
        per_device, mesh=mesh, in_specs=in_specs, out_specs=out_specs, check_vma=False
    )
```

profile of v0, /device:TPU:0, one launch (start us, length us, event | category | flops | bytes accessed | tf_op | source)
XLA Modules:
  0.0 333.9 jit_solution(18437636033774966400)
XLA Ops:
  6.5 0.7 all-gather.2.cloned.1.call-update
  7.3 33.6 %all_gather.12 = bf16[2048,1,128]{2,0,1:T(8,128)(2,1)S(1)} all-gather(bf16[256,1,128]{2,0,1:T(8,128)(2,1)} %param.22), channel_id=1, replica_groups=mesh['sp'=8,'tp'=4] {'sp'}, dimensions={0}, use_global_device_ids=true | all-gather | bytes 589824 | tf_op jit(solution)/shard_map/all_gather | solution.py:107
  40.9 0.8 copy.35
  44.2 2.8 fusion.88
  47.0 1.8 fusion.89
  48.9 31.4 %all_gather.15 = bf16[2048,1,128]{2,0,1:T(8,128)(2,1)S(1)} all-gather(bf16[256,1,128]{2,0,1:T(8,128)(2,1)S(1)} %copy-done.5), channel_id=1, replica_groups=mesh['sp'=8,'tp'=4] {'sp'}, dimensions={0}, use_global_device_ids=true | all-gather | bytes 589824 | tf_op jit(solution)/shard_map/all_gather | solution.py:110
  80.3 31.5 %all_gather.13 = bf16[2048,1,128]{2,0,1:T(8,128)(2,1)S(1)} all-gather(bf16[256,1,128]{2,0,1:T(8,128)(2,1)S(1)} %copy-done.6), channel_id=1, replica_groups=mesh['sp'=8,'tp'=4] {'sp'}, dimensions={0}, use_global_device_ids=true | all-gather | bytes 589824 | tf_op jit(solution)/shard_map/all_gather | solution.py:108
  111.8 1.8 fusion.91
  113.6 1.8 fusion.90
  115.4 2.1 fusion.19
  121.0 0.7 reduce.22
  122.5 3.3 all-to-all-start.1
  125.8 0.7 reduce.23
  127.3 2.6 all-to-all-done.1
  129.9 3.3 all-to-all-start
  133.3 3.9 %all-to-all-done = bf16[4,2,4096]{2,1,0:T(2,128)(2,1)S(1)} async-done(((bf16[4,2,4096]{2,1,0:T(2,128)(2,1)}), bf16[4,2,4096]{2,1,0:T(2,128)(2,1)S(1)}, u32[]{:S(2)}, u32[]{:S(2)}) %all-to-all-start) | async-done | bytes 65568 | tf_op jit(solution)/shard_map/all_to_all | solution.py:139
  137.4 3.2 multiply_reduce_fusion.1
  140.7 2.3 gather_fusion
  143.1 1.6 broadcast_in_dim.49
  144.7 46.2 %scatter_fusion = bf16[32,16,2048]{2,1,0:T(8,128)(2,1)} fusion(bf16[32,16,2048]{2,1,0:T(8,128)(2,1)} %broadcast_in_dim.49, s32[256]{0:T(256)S(1)} %bitcast.169, bf16[256,2048]{1,0:T(8,128)(2,1)} %gather_fusion), kind=kCustom, calls=%fused_computation.2 | custom fusion | bytes 3147776 | tf_op jit(solution)/shard_map/scatter | solution.py:168
  190.9 53.7 %all_to_all.40 = bf16[32,16,2048]{2,1,0:T(8,128)(2,1)S(1)} all-to-all(bf16[32,16,2048]{2,1,0:T(8,128)(2,1)} %scatter_fusion), channel_id=1, replica_groups=mesh['sp'=8,'tp'=4] {'sp','tp'}, dimensions={0} | all-to-all | bytes 4194304 | tf_op jit(solution)/shard_map/all_to_all | solution.py:170
  244.6 1.3 copy-done.3
  246.0 3.6 %fusion.4 = f32[512,1024]{1,0:T(8,128)} fusion(bf16[512,2048]{1,0:T(8,128)(2,1)S(1)} %bitcast.171, bf16[1,2048,1024]{2,1,0:T(8,128)(2,1)S(1)} %copy-done.10), kind=kOutput, calls=%fused_computation.7 | convolution fusion | flops 2147483648 | bytes 8388608 | tf_op jit(solution)/shard_map/dot_general | solution.py:14
  249.6 10.6 %fusion.6 = bf16[512,2048]{1,0:T(8,128)(2,1)} fusion(bf16[1,1024,2048]{2,1,0:T(8,128)(2,1)} %param.36, f32[512,1024]{1,0:T(8,128)} %fusion.4, bf16[512,2048]{1,0:T(8,128)(2,1)} %bitcast.172, bf16[1,2048,1024]{2,1,0:T(8,128)(2,1)} %param.35), kind=kOutput, calls=%fused_computation.9 | convolution fusion | flops 4299161600 | bytes 14680064 | tf_op jit(solution)/shard_map/dot_general | solution.py:17
  260.2 3.8 %all-to-all-start.3 = ((bf16[32,16,2048]{2,1,0:T(8,128)(2,1)}), bf16[32,16,2048]{2,1,0:T(8,128)(2,1)}, u32[]{:S(2)}, u32[]{:S(2)}) async-start(bf16[32,16,2048]{2,1,0:T(8,128)(2,1)} %bitcast.170), calls=%async_computation.3 | async-start | bytes 4194304 | tf_op jit(solution)/shard_map/all_to_all | solution.py:177
  264.0 0.7 copy.39
  264.7 2.1 fusion.92
  266.8 45.9 %all-to-all-done.3 = bf16[32,16,2048]{2,1,0:T(8,128)(2,1)} async-done(((bf16[32,16,2048]{2,1,0:T(8,128)(2,1)}), bf16[32,16,2048]{2,1,0:T(8,128)(2,1)}, u32[]{:S(2)}, u32[]{:S(2)}) %all-to-all-start.3) | async-done | bytes 2097184 | tf_op jit(solution)/shard_map/all_to_all | solution.py:177
  312.7 5.1 %gather_fusion.1 = bf16[256,2048]{1,0:T(8,128)(2,1)} fusion(bf16[32,16,2048]{2,1,0:T(8,128)(2,1)} %all-to-all-done.3, s32[256]{0:T(256)S(1)} %bitcast.168), kind=kCustom, calls=%fused_computation.1 | custom fusion | bytes 2099200 | tf_op jit(solution)/shard_map/gather | solution.py:178
  317.9 2.7 reshape.410
  320.6 3.2 multiply_reduce_fusion
  323.8 3.2 fusion.14
  (68 shorter events, 6.7 us)
Async XLA Ops:
  6.5 317.3 %copy-start = (bf16[512,2048]{1,0:T(8,128)(2,1)S(1)}, bf16[512,2048]{1,0:T(8,128)(2,1)}, u32[]{:S(2)}) copy-start(bf16[512,2048]{1,0:T(8,128)(2,1)} %param.39) | copy-start | bytes 6291460
  6.5 40.5 %copy-start.12 = (bf16[256,1,128]{2,0,1:T(8,128)(2,1)S(1)}, bf16[256,1,128]{2,0,1:T(8,128)(2,1)}, u32[]{:S(2)}) copy-start(bf16[256,1,128]{2,0,1:T(8,128)(2,1)} %param.21) | copy-start | bytes 196612
  6.5 105.2 %all-gather.2.cloned.1.call-start = ((), (), s32[]{:S(2)}) async-start(), calls=%async_computation.4 | async-start | bytes 1179648 | tf_op jit(solution)/shard_map/all_gather | solution.py:109
  47.0 1.9 copy-start.5
  47.0 33.3 %copy-start.6 = (bf16[256,1,128]{2,0,1:T(8,128)(2,1)S(1)}, bf16[256,1,128]{2,0,1:T(8,128)(2,1)}, u32[]{:S(2)}) copy-start(bf16[256,1,128]{2,0,1:T(8,128)(2,1)} %param.23) | copy-start | bytes 196612
  47.0 64.8 %copy-start.11 = (bf16[256,1,256]{2,0,1:T(8,128)(2,1)S(1)}, bf16[256,1,256]{2,0,1:T(8,128)(2,1)}, u32[]{:S(2)}) copy-start(bf16[256,1,256]{2,0,1:T(8,128)(2,1)} %param.24) | copy-start | bytes 393220
  111.8 3.6 %copy-start.2 = (f32[256,2048]{1,0:T(8,128)S(1)}, f32[256,2048]{1,0:T(8,128)}, u32[]{:S(2)}) copy-start(f32[256,2048]{1,0:T(8,128)} %get-tuple-element.62) | copy-start | bytes 6291460
  113.6 1.8 copy-start.1
  119.6 0.7 copy-start.9
  120.3 17.1 %copy-start.4 = (bf16[64,2048]{1,0:T(8,128)(2,1)S(1)}, bf16[64,2048]{1,0:T(8,128)(2,1)}, u32[]{:S(2)}) copy-start(bf16[64,2048]{1,0:T(8,128)(2,1)} %param.20) | copy-start | bytes 786436
  122.5 7.4 %all-to-all-start.1 = ((bf16[4,2,4096]{2,1,0:T(2,128)(2,1)}), bf16[4,2,4096]{2,1,0:T(2,128)(2,1)S(1)}, u32[]{:S(2)}, u32[]{:S(2)}) async-start(bf16[4,2,4096]{2,1,0:T(2,128)(2,1)} %reshape.432), calls=%async_computation.1 | async-start | bytes 131072 | tf_op jit(solution)/shard_map/all_to_all | solution.py:140
  129.9 7.4 %all-to-all-start = ((bf16[4,2,4096]{2,1,0:T(2,128)(2,1)}), bf16[4,2,4096]{2,1,0:T(2,128)(2,1)S(1)}, u32[]{:S(2)}, u32[]{:S(2)}) async-start(bf16[4,2,4096]{2,1,0:T(2,128)(2,1)} %reshape.434), calls=%async_computation | async-start | bytes 131072 | tf_op jit(solution)/shard_map/all_to_all | solution.py:139
  137.4 3.2 copy-start.7
  190.9 55.0 %copy-start.10 = (bf16[1,2048,1024]{2,1,0:T(8,128)(2,1)S(1)}, bf16[1,2048,1024]{2,1,0:T(8,128)(2,1)}, u32[]{:S(2)}) copy-start(bf16[1,2048,1024]{2,1,0:T(8,128)(2,1)} %param.34) | copy-start | bytes 12582916
  244.6 1.3 copy-start.3
  260.2 3.8 %copy-start.8 = (f32[64,4]{0,1:T(4,128)S(1)}, f32[64,4]{0,1:T(4,128)}, u32[]{:S(2)}) copy-start(f32[64,4]{0,1:T(4,128)} %param.33) | copy-start | bytes 3076
  260.2 52.5 %all-to-all-start.3 = ((bf16[32,16,2048]{2,1,0:T(8,128)(2,1)}), bf16[32,16,2048]{2,1,0:T(8,128)(2,1)}, u32[]{:S(2)}, u32[]{:S(2)}) async-start(bf16[32,16,2048]{2,1,0:T(8,128)(2,1)} %bitcast.170), calls=%async_computation.3 | async-start | bytes 4194304 | tf_op jit(solution)/shard_map/all_to_all | solution.py:177
Sparse Core Ops, SparseCore 0:
  9.5 43.6 all-gather.1
where the time goes:
time: 336 us; the launch traced here: 334 us
  blocking collectives  150 us (45%)
  local copies, waits for them, and re-layouts  63.9 us (19%)
  waiting for transfers between devices  53.1 us (16%)
  matrix products  33.6 us (10%)
  between operations  15.1 us (4%)
  starting transfers between devices  10.4 us (3%)
  other arithmetic  7.7 us (2%)
    all_to_all x1, blocking collectives, per_device(): lax.all_to_all(send_rows, ('sp', 'tp'), split_axis=0, concat_axis=0, tile...  53.7 us
    scatter x1, local copies, waits for them, and re-layouts, per_device(): send_rows = jnp.zeros((expert_total, capacity, model_width), jnp.bfloat16...  46.2 us
    all_to_all x1, waiting for transfers between devices, per_device(): lax.all_to_all(finished, ('sp', 'tp'), split_axis=0, concat_axis=0, tiled...  45.9 us
    all_gather x1, blocking collectives, per_device(): key_piece_a = lax.all_gather(key_a, 'sp', axis=0, tiled=True)  33.6 us
    all_gather x1, blocking collectives, per_device(): value_piece_a = lax.all_gather(value_a, 'sp', axis=0, tiled=True)  31.5 us
    all_gather x1, blocking collectives, per_device(): value_piece_b = lax.all_gather(value_b, 'sp', axis=0, tiled=True)  31.4 us
    dot_general x2, matrix products, swiglu_rows(): return jnp.dot(hidden, w_down, preferred_element_type=jnp.float32)  13.8 us
    dot_general x4, matrix products, online_update(): jnp.einsum('qhd,khd->hqk', query_map, key_map, preferred_element_type=jnp...  8.17 us
  transfers between devices with their start and end apart: 4, of which 3 were waited for; matrix products, arithmetic and copies ran while one was open for 3% of the time, Pallas kernels for 0%

commit v1 on v0

--- a/solution.py
+++ b/solution.py
@@ -8,6 +8,28 @@
 EPSILON = 1e-05
 HEAD_SCALE = 0.8
 KEY_SPAN = 2048
+
+
+def in_order(blocks, dim):
+    blocks = jnp.moveaxis(blocks, 0, dim)
+    shape = blocks.shape
+    return blocks.reshape(*shape[:dim], shape[dim] * shape[dim + 1], *shape[dim + 2 :])
+
+
+def collected_by_bits(value, axis):
+    peers = lax.axis_size(axis)
+    tiles = value[None]
+    for level in range(peers.bit_length() - 1):
+        bit = 1 << level
+        theirs = lax.ppermute(tiles, axis, [(i, i ^ bit) for i in range(peers)])
+        both = jnp.stack([tiles, theirs])
+        upper = lax.axis_index(axis) >> level & 1
+        tiles = jnp.where(upper == 0, both, both[::-1]).reshape(-1, *value.shape)
+    return tiles
+
+
+def collect(x, axis, dim):
+    return in_order(collected_by_bits(x, axis), dim)
 
 
 def swiglu_rows(row_set, w_gate, w_up, w_down):
@@ -107,7 +129,7 @@
     key_piece_a = lax.all_gather(key_a, "sp", axis=0, tiled=True)
     value_piece_a = lax.all_gather(value_a, "sp", axis=0, tiled=True)
     key_piece_b = lax.all_gather(key_b, "sp", axis=0, tiled=True)
-    value_piece_b = lax.all_gather(value_b, "sp", axis=0, tiled=True)
+    value_piece_b = collect(value_b, "sp", 0)
     piece_rows = key_piece_a.shape[0]
     step_rows = math.gcd(piece_rows, KEY_SPAN)
 

time: 336 us -> 311 us (0.926)
  blocking collectives: 150 us -> 116 us
  waiting for transfers between devices: 53.1 us -> 59.6 us
  starting transfers between devices: 10.4 us -> 13.9 us
    all_gather x1 -> x0, blocking collectives: 31.4 us -> none  [per_device(): value_piece_b = lax.all_gather(value_b, 'sp', axis=0, tiled=True)]
    ppermute x0 -> x3, waiting for transfers between devices: none -> 6.43 us  [collected_by_bits(): theirs = lax.ppermute(tiles, axis, [(i, i ^ bit) for i in range(peers)])]
    ppermute x0 -> x3, starting transfers between devices: none -> 3.62 us  [collected_by_bits(): theirs = lax.ppermute(tiles, axis, [(i, i ^ bit) for i in range(peers)])]
  transfers between devices with their start and end apart: 4 -> 7, of which waited for: 3 -> 4; matrix products, arithmetic and copies ran while one was open for 3% -> 3% of each run, Pallas kernels for 0% -> 0%
where the time goes in v1:
time: 311 us; the launch traced here: 309 us
  blocking collectives  116 us (37%)
  local copies, waits for them, and re-layouts  63.2 us (20%)
  waiting for transfers between devices  59.6 us (19%)
  matrix products  33.5 us (11%)
  between operations  15.2 us (5%)
  starting transfers between devices  13.9 us (4%)
  other arithmetic  8 us (3%)
    all_to_all x1, blocking collectives, per_device(): lax.all_to_all(send_rows, ('sp', 'tp'), split_axis=0, concat_axis=0, tile...  51.9 us
    scatter x1, local copies, waits for them, and re-layouts, per_device(): send_rows = jnp.zeros((expert_total, capacity, model_width), jnp.bfloat16...  46.2 us
    all_to_all x1, waiting for transfers between devices, per_device(): lax.all_to_all(finished, ('sp', 'tp'), split_axis=0, concat_axis=0, tiled...  45.9 us
    all_gather x1, blocking collectives, per_device(): key_piece_a = lax.all_gather(key_a, 'sp', axis=0, tiled=True)  32.4 us
    all_gather x1, blocking collectives, per_device(): value_piece_a = lax.all_gather(value_a, 'sp', axis=0, tiled=True)  31.4 us
    dot_general x2, matrix products, swiglu_rows(): return jnp.dot(hidden, w_down, preferred_element_type=jnp.float32)  13.8 us
    dot_general x4, matrix products, online_update(): jnp.einsum('qhd,khd->hqk', query_map, key_map, preferred_element_type=jnp...  8.19 us
    ppermute x3, waiting for transfers between devices, collected_by_bits(): theirs = lax.ppermute(tiles, axis, [(i, i ^ bit) for i in range(peers)])  6.43 us
  transfers between devices with their start and end apart: 7, of which 4 were waited for; matrix products, arithmetic and copies ran while one was open for 3% of the time, Pallas kernels for 0%

profile of v1, /device:TPU:0, one launch (start us, length us, event | category | flops | bytes accessed | tf_op | source)
XLA Modules:
  0.0 309.1 jit_solution(6332808354653380813)
XLA Ops:
  6.5 0.7 all-gather.2.cloned.1.call-update
  7.3 3.1 collective-permute-start
  10.3 32.4 %all_gather.9 = bf16[2048,1,128]{2,0,1:T(8,128)(2,1)S(1)} all-gather(bf16[256,1,128]{2,0,1:T(8,128)(2,1)} %param.22), channel_id=1, replica_groups=mesh['sp'=8,'tp'=4] {'sp'}, dimensions={0}, use_global_device_ids=true | all-gather | bytes 589824 | tf_op jit(solution)/shard_map/all_gather | solution.py:129
  42.8 2.8 fusion.88
  45.6 1.8 fusion.89
  49.0 6.4 %collective-permute-done.1 = bf16[2,256,1,128]{3,1,0,2:T(8,128)(2,1)S(1)} collective-permute-done((bf16[2,256,1,128]{3,1,0,2:T(8,128)(2,1)S(1)}, bf16[2,256,1,128]{3,1,0,2:T(8,128)(2,1)S(1)}, u32[]{:S(2)}, u32[]{:S(2)}) %collective-permute-start.1) | collective-permute-done | bytes 131104 | tf_op jit(solution)/shard_map/ppermute | solution.py:24
  57.3 31.4 %all_gather.10 = bf16[2048,1,128]{2,0,1:T(8,128)(2,1)S(1)} all-gather(bf16[256,1,128]{2,0,1:T(8,128)(2,1)S(1)} %copy-done.5), channel_id=1, replica_groups=mesh['sp'=8,'tp'=4] {'sp'}, dimensions={0}, use_global_device_ids=true | all-gather | bytes 589824 | tf_op jit(solution)/shard_map/all_gather | solution.py:130
  88.9 1.8 fusion.91
  90.7 1.8 fusion.90
  92.6 2.1 fusion.19
  98.1 0.7 reduce.22
  99.6 3.3 %all-to-all-start.1 = ((bf16[4,2,4096]{2,1,0:T(2,128)(2,1)}), bf16[4,2,4096]{2,1,0:T(2,128)(2,1)S(1)}, u32[]{:S(2)}, u32[]{:S(2)}) async-start(bf16[4,2,4096]{2,1,0:T(2,128)(2,1)} %reshape.442), calls=%async_computation.1 | async-start | bytes 131072 | tf_op jit(solution)/shard_map/all_to_all | solution.py:162
  102.9 0.7 reduce.23
  104.3 2.6 all-to-all-done.1
  106.9 3.3 %all-to-all-start = ((bf16[4,2,4096]{2,1,0:T(2,128)(2,1)}), bf16[4,2,4096]{2,1,0:T(2,128)(2,1)S(1)}, u32[]{:S(2)}, u32[]{:S(2)}) async-start(bf16[4,2,4096]{2,1,0:T(2,128)(2,1)} %reshape.444), calls=%async_computation | async-start | bytes 131072 | tf_op jit(solution)/shard_map/all_to_all | solution.py:161
  110.4 3.9 %all-to-all-done = bf16[4,2,4096]{2,1,0:T(2,128)(2,1)S(1)} async-done(((bf16[4,2,4096]{2,1,0:T(2,128)(2,1)}), bf16[4,2,4096]{2,1,0:T(2,128)(2,1)S(1)}, u32[]{:S(2)}, u32[]{:S(2)}) %all-to-all-start) | async-done | bytes 65568 | tf_op jit(solution)/shard_map/all_to_all | solution.py:161
  114.5 3.2 %multiply_reduce_fusion.1 = (f32[64]{0:T(128)S(1)}, f32[64,2048]{1,0:T(8,128)S(1)}) fusion(bf16[1024,2048]{1,0:T(8,128)(2,1)} %param.30, bf16[64,512]{1,0:T(8,128)(2,1)S(1)} %bitcast.180, bf16[64,512]{1,0:T(8,128)(2,1)S(1)} %bitcast.181, bf16[64,2048]{1,0:T(8,128)(2,1)S(1)} %copy-done.4), kind=kOutput, calls=%fused_computation.68 | convolution fusion | flops 269483968 | bytes 5112064 | tf_op jit(solution)/shard_map/dot_general | solution.py:165
  117.8 2.3 gather_fusion
  120.2 1.6 broadcast_in_dim.53
  121.8 46.2 %scatter_fusion = bf16[32,16,2048]{2,1,0:T(8,128)(2,1)} fusion(bf16[32,16,2048]{2,1,0:T(8,128)(2,1)} %broadcast_in_dim.53, s32[256]{0:T(256)S(1)} %bitcast.172, bf16[256,2048]{1,0:T(8,128)(2,1)} %gather_fusion), kind=kCustom, calls=%fused_computation.2 | custom fusion | bytes 3147776 | tf_op jit(solution)/shard_map/scatter | solution.py:190
  168.0 51.9 %all_to_all.40 = bf16[32,16,2048]{2,1,0:T(8,128)(2,1)S(1)} all-to-all(bf16[32,16,2048]{2,1,0:T(8,128)(2,1)} %scatter_fusion), channel_id=1, replica_groups=mesh['sp'=8,'tp'=4] {'sp','tp'}, dimensions={0} | all-to-all | bytes 4194304 | tf_op jit(solution)/shard_map/all_to_all | solution.py:192
  219.9 1.3 copy-done.3
  221.3 3.6 %fusion.4 = f32[512,1024]{1,0:T(8,128)} fusion(bf16[512,2048]{1,0:T(8,128)(2,1)S(1)} %bitcast.174, bf16[1,2048,1024]{2,1,0:T(8,128)(2,1)S(1)} %copy-done.11), kind=kOutput, calls=%fused_computation.7 | convolution fusion | flops 2147483648 | bytes 8388608 | tf_op jit(solution)/shard_map/dot_general | solution.py:36
  224.9 10.6 %fusion.6 = bf16[512,2048]{1,0:T(8,128)(2,1)} fusion(bf16[1,1024,2048]{2,1,0:T(8,128)(2,1)} %param.36, f32[512,1024]{1,0:T(8,128)} %fusion.4, bf16[512,2048]{1,0:T(8,128)(2,1)} %bitcast.175, bf16[1,2048,1024]{2,1,0:T(8,128)(2,1)} %param.35), kind=kOutput, calls=%fused_computation.9 | convolution fusion | flops 4299161600 | bytes 14680064 | tf_op jit(solution)/shard_map/dot_general | solution.py:39
  235.5 3.7 %all-to-all-start.3 = ((bf16[32,16,2048]{2,1,0:T(8,128)(2,1)}), bf16[32,16,2048]{2,1,0:T(8,128)(2,1)}, u32[]{:S(2)}, u32[]{:S(2)}) async-start(bf16[32,16,2048]{2,1,0:T(8,128)(2,1)} %bitcast.173), calls=%async_computation.3 | async-start | bytes 4194304 | tf_op jit(solution)/shard_map/all_to_all | solution.py:199
  239.2 0.7 copy.39
  239.9 2.1 fusion.92
  242.0 45.9 %all-to-all-done.3 = bf16[32,16,2048]{2,1,0:T(8,128)(2,1)} async-done(((bf16[32,16,2048]{2,1,0:T(8,128)(2,1)}), bf16[32,16,2048]{2,1,0:T(8,128)(2,1)}, u32[]{:S(2)}, u32[]{:S(2)}) %all-to-all-start.3) | async-done | bytes 2097184 | tf_op jit(solution)/shard_map/all_to_all | solution.py:199
  287.9 5.1 %gather_fusion.1 = bf16[256,2048]{1,0:T(8,128)(2,1)} fusion(bf16[32,16,2048]{2,1,0:T(8,128)(2,1)} %all-to-all-done.3, s32[256]{0:T(256)S(1)} %bitcast.171), kind=kCustom, calls=%fused_computation.1 | custom fusion | bytes 2099200 | tf_op jit(solution)/shard_map/gather | solution.py:200
  293.1 2.7 reshape.420
  295.8 3.2 %multiply_reduce_fusion = f32[64,2048]{1,0:T(8,128)S(1)} fusion(f32[64,4,2048]{2,1,0:T(4,128)} %reshape.420, f32[64,4]{1,0:T(8,128)} %copy.39), kind=kLoop, calls=%fused_computation.24 | loop fusion | flops 917504 | bytes 2622464 | tf_op jit(solution)/shard_map/reduce_sum | solution.py:201
  299.0 3.2 %fusion.14 = bf16[64,2048]{1,0:T(8,128)(2,1)} fusion(f32[64,2048]{1,0:T(8,128)S(1)} %multiply_reduce_fusion, f32[64,2048]{1,0:T(8,128)S(1)} %get-tuple-element.99, bf16[512,2048]{1,0:T(8,128)(2,1)S(1)} %copy-done, bf16[64,2048]{1,0:T(8,128)(2,1)S(1)} %multiply_convert_fusion.1, bf16[2048,512]{1,0:T(8,128)(2,1)} %param.38, f32[64,512]{1,0:T(8,128)S(1)} %fusion.92), kind=kOutput, calls=%fused_computation.21 | convolution fusion | flops 269025280 | bytes 5898240 | tf_op jit(solution)/shard_map/dot_general | solution.py:39
  (81 shorter events, 7.6 us)
Async XLA Ops:
  6.5 292.5 %copy-start = (bf16[512,2048]{1,0:T(8,128)(2,1)S(1)}, bf16[512,2048]{1,0:T(8,128)(2,1)}, u32[]{:S(2)}) copy-start(bf16[512,2048]{1,0:T(8,128)(2,1)} %param.39) | copy-start | bytes 6291460
  6.5 39.0 %copy-start.13 = (bf16[256,1,128]{2,0,1:T(8,128)(2,1)S(1)}, bf16[256,1,128]{2,0,1:T(8,128)(2,1)}, u32[]{:S(2)}) copy-start(bf16[256,1,128]{2,0,1:T(8,128)(2,1)} %param.21) | copy-start | bytes 196612
  6.5 82.4 %all-gather.2.cloned.1.call-start = ((), (), s32[]{:S(2)}) async-start(), calls=%async_computation.4 | async-start | bytes 1179648 | tf_op jit(solution)/shard_map/all_gather | solution.py:131
  7.3 41.5 %collective-permute-start = (bf16[1,256,1,128]{3,1,2,0:T(8,128)(2,1)}, bf16[1,256,1,128]{3,1,2,0:T(8,128)(2,1)S(1)}, u32[]{:S(2)}, u32[]{:S(2)}) collective-permute-start(bf16[1,256,1,128]{3,1,2,0:T(8,128)(2,1)} %bitcast.188), channel_id=1, source_target_pairs={{0,4},{4,0},{8,12},{12,8},{16,20},{20,16},{24,28},{28,24},{1,5},{5... | collective-permute-start | bytes 196616 | tf_op jit(solution)/shard_map/ppermute | solution.py:24
  45.5 1.8 copy-start.8
  45.5 3.2 %copy-start.6 = (bf16[256,1,128]{2,0,1:T(8,128)(2,1)S(1)}, bf16[256,1,128]{2,0,1:T(8,128)(2,1)}, u32[]{:S(2)}) copy-start(bf16[256,1,128]{2,0,1:T(8,128)(2,1)} %param.26) | copy-start | bytes 196612
  45.6 11.7 %copy-start.5 = (bf16[256,1,128]{2,0,1:T(8,128)(2,1)S(1)}, bf16[256,1,128]{2,0,1:T(8,128)(2,1)}, u32[]{:S(2)}) copy-start(bf16[256,1,128]{2,0,1:T(8,128)(2,1)} %param.23) | copy-start | bytes 196612
  48.9 6.5 %collective-permute-start.1 = (bf16[2,256,1,128]{3,1,0,2:T(8,128)(2,1)S(1)}, bf16[2,256,1,128]{3,1,0,2:T(8,128)(2,1)S(1)}, u32[]{:S(2)}, u32[]{:S(2)}) collective-permute-start(bf16[2,256,1,128]{3,1,0,2:T(8,128)(2,1)S(1)} %get-tuple-element.52), channel_id=1, source_target_pairs={{0,8},{4,12},{8,0},{12,4},{16,24},{20,28},{24,16},{28,20},{1,9},{5... | collective-permute-start | bytes 393224 | tf_op jit(solution)/shard_map/ppermute | solution.py:24
  55.5 33.2 %collective-permute-start.2 = (bf16[4,256,1,128]{3,1,0,2:T(8,128)(2,1)S(1)}, bf16[4,256,1,128]{3,1,0,2:T(8,128)(2,1)S(1)}, u32[]{:S(2)}, u32[]{:S(2)}) collective-permute-start(bf16[4,256,1,128]{3,1,0,2:T(8,128)(2,1)S(1)} %bitcast.176), channel_id=1, source_target_pairs={{0,16},{4,20},{8,24},{12,28},{16,0},{20,4},{24,8},{28,12},{1,17},{... | collective-permute-start | bytes 786440 | tf_op jit(solution)/shard_map/ppermute | solution.py:24
  88.7 2.0 copy-start.12
  88.9 3.6 %copy-start.2 = (f32[256,2048]{1,0:T(8,128)S(1)}, f32[256,2048]{1,0:T(8,128)}, u32[]{:S(2)}) copy-start(f32[256,2048]{1,0:T(8,128)} %get-tuple-element.86) | copy-start | bytes 6291460
  90.7 1.8 copy-start.1
  96.6 0.7 copy-start.10
  97.3 17.1 %copy-start.4 = (bf16[64,2048]{1,0:T(8,128)(2,1)S(1)}, bf16[64,2048]{1,0:T(8,128)(2,1)}, u32[]{:S(2)}) copy-start(bf16[64,2048]{1,0:T(8,128)(2,1)} %param.20) | copy-start | bytes 786436
  99.6 7.4 %all-to-all-start.1 = ((bf16[4,2,4096]{2,1,0:T(2,128)(2,1)}), bf16[4,2,4096]{2,1,0:T(2,128)(2,1)S(1)}, u32[]{:S(2)}, u32[]{:S(2)}) async-start(bf16[4,2,4096]{2,1,0:T(2,128)(2,1)} %reshape.442), calls=%async_computation.1 | async-start | bytes 131072 | tf_op jit(solution)/shard_map/all_to_all | solution.py:162
  106.9 7.4 %all-to-all-start = ((bf16[4,2,4096]{2,1,0:T(2,128)(2,1)}), bf16[4,2,4096]{2,1,0:T(2,128)(2,1)S(1)}, u32[]{:S(2)}, u32[]{:S(2)}) async-start(bf16[4,2,4096]{2,1,0:T(2,128)(2,1)} %reshape.444), calls=%async_computation | async-start | bytes 131072 | tf_op jit(solution)/shard_map/all_to_all | solution.py:161
  114.5 3.2 %copy-start.7 = (f32[2048]{0:T(1024)S(1)}, f32[2048]{0:T(1024)}, u32[]{:S(2)}) copy-start(f32[2048]{0:T(1024)} %param.31) | copy-start | bytes 24580
  168.0 53.2 %copy-start.11 = (bf16[1,2048,1024]{2,1,0:T(8,128)(2,1)S(1)}, bf16[1,2048,1024]{2,1,0:T(8,128)(2,1)}, u32[]{:S(2)}) copy-start(bf16[1,2048,1024]{2,1,0:T(8,128)(2,1)} %param.34) | copy-start | bytes 12582916
  219.9 1.3 copy-start.3
  235.5 3.7 %copy-start.9 = (f32[64,4]{0,1:T(4,128)S(1)}, f32[64,4]{0,1:T(4,128)}, u32[]{:S(2)}) copy-start(f32[64,4]{0,1:T(4,128)} %param.33) | copy-start | bytes 3076
  235.5 52.4 %all-to-all-start.3 = ((bf16[32,16,2048]{2,1,0:T(8,128)(2,1)}), bf16[32,16,2048]{2,1,0:T(8,128)(2,1)}, u32[]{:S(2)}, u32[]{:S(2)}) async-start(bf16[32,16,2048]{2,1,0:T(8,128)(2,1)} %bitcast.173), calls=%async_computation.3 | async-start | bytes 4194304 | tf_op jit(solution)/shard_map/all_to_all | solution.py:199
Sparse Core Ops, SparseCore 0:
  9.5 43.9 all-gather.1
